TPU v7x, 32 devices: a whole 2x2x4 slice. The times are simulated.
32 devices in a mesh: rep: 8 (over z, y), fs: 2 (over x), tp: 2 (over core).
Axes of the slice: x: 2, y: 2, z: 4, core: 2. Of those that a mesh axis runs over, the one named last changes fastest.
Arguments:
- inputs: bfloat16 [4096, 2048], P(('rep', 'tp'), 'fs'), may hold values from -6 to 6
- pre_act: bfloat16 [4096, 4096], P(('rep', 'fs'), 'tp'), may hold values from -6 to 6
- cotangent: bfloat16 [4096, 2048], P(('rep', 'tp'), 'fs'), may hold values from -6 to 6
- up_weight: bfloat16 [2048, 4096], P('fs', 'tp'), may hold values from -0.125 to 0.125
- down_weight: bfloat16 [4096, 2048], P('tp', 'fs'), may hold values from -0.09375 to 0.09375
Outputs:
- grad_inputs: bfloat16 [4096, 2048], P(('rep', 'tp'), 'fs')
- grad_up: float32 [2048, 4096], P('fs', 'tp')
- grad_down: float32 [4096, 2048], P('tp', 'fs')
All inputs are finite; a program needn't handle non-finite values.
Results may differ from a plain program's by a relative error of at most 0.015.
Values may be sent and summed in bfloat16 or wider, within the bound.
A program may use at most 128 MiB of HBM per device.

v0:
```python
import functools

import jax
import jax.numpy as jnp
from jax import lax
from jax.experimental import pallas as pl
from jax.experimental.pallas import tpu as pltpu
from jax.sharding import PartitionSpec as P

MESH = pl.DeviceIdType.MESH
LANES = 128
F32, BF16 = jnp.float32, jnp.bfloat16


def rows_dot(left, right):
    return lax.dot_general(left, right, (((0,), (0,)), ((), ())), preferred_element_type=F32)


def cols_dot(left, right):
    return lax.dot_general(left, right, (((1,), (1,)), ((), ())), preferred_element_type=F32)


def plan(n_rep, width, hidden):
    panels = hidden // LANES
    room = width * panels // (2 * n_rep)
    subs = max(n for n in (1, 2) if n == 1 or room // n >= 2 * LANES)
    per_panel = 2 * n_rep * subs // panels
    return subs, per_panel, width // per_panel


def kernel(
    n_rep, x_hbm, pre_hbm, cot_hbm, wu_hbm, wd_hbm,
    gi_ref, up_ref, down_ref,
    x_ref, pre_ref, cot_ref, wu, wd, xg, cg, pre_in, sq, gp, pa_own, pa_out, pa_in, gi_out, gi_in,
    first_d, first_u, rs_d, rs_u,
    w_sem, tp_s, tp_r, pre_s, pre_r, gp_s, gp_r, pa_s, pa_r, gi_s, gi_r,
    rsd_s, rsd_r, rsu_s, rsu_r, agd_s, agd_r, agu_s, agu_r,
):
    half, width = x_ref.shape
    hidden = pre_ref.shape[1]
    panels = hidden // LANES
    subs, per_panel, w = plan(n_rep, width, hidden)
    fine = 2 * n_rep == panels
    rep, fs, tp = lax.axis_index("rep"), lax.axis_index("fs"), lax.axis_index("tp")
    line = n_rep // 2
    row, col = rep // 2, rep % 2
    pos = jnp.where(col == 0, row, n_rep - 1 - row)

    def rep_at(p):
        p = lax.rem(p + n_rep, n_rep)
        return jnp.where(p < line, 2 * p, 2 * (n_rep - 1 - p) + 1)

    nxt, prv = rep_at(pos + 1), rep_at(pos + n_rep - 1)
    goal = ({"rep": nxt}, {"rep": prv})
    other_fs, other_tp = {"fs": 1 - fs}, {"tp": 1 - tp}
    mine_f = pl.ds(pl.multiple_of(fs * half, half), half)
    his_f = pl.ds(pl.multiple_of((1 - fs) * half, half), half)
    mine_t = pl.ds(pl.multiple_of(tp * half, half), half)
    his_t = pl.ds(pl.multiple_of((1 - tp) * half, half), half)

    def remote(src, dst, s, r, dev):
        return pltpu.make_async_remote_copy(
            src_ref=src, dst_ref=dst, send_sem=s, recv_sem=r, device_id=dev,
            device_id_type=MESH)

    barrier = pltpu.get_barrier_semaphore()
    for dev in (goal[0], goal[1], other_fs, other_tp):
        pl.semaphore_signal(barrier, inc=1, device_id=dev, device_id_type=MESH)
    held = ((cot_hbm, cot_ref), (pre_hbm, pre_ref), (x_hbm, x_ref), (wd_hbm, wd), (wu_hbm, wu))
    loads = [pltpu.make_async_copy(src, dst, w_sem.at[i]) for i, (src, dst) in enumerate(held)]
    load_cot, load_pre, load_x, load_wd, load_wu = loads
    for load in loads:
        load.start()
    load_cot.wait()
    load_pre.wait()
    pl.semaphore_wait(barrier, 4)

    def chunk_of(d, j):
        return lax.rem(pos + (-1 - j if d == 0 else 1 + j) + 2 * n_rep, n_rep)

    def lanes(panel):
        return pl.ds(pl.multiple_of(panel * LANES, LANES), LANES)

    def panel_of(d, j):
        return d * n_rep + chunk_of(d, j)

    def pre_copy(panel):
        return remote(pre_ref.at[:, lanes(panel)], pre_in.at[:, lanes(panel)],
                      pre_s.at[panel], pre_r.at[panel], other_fs)

    def gp_copy(panel):
        return remote(gp.at[mine_f, lanes(panel)], gp.at[mine_f, lanes(panel)],
                      gp_s.at[panel], gp_r.at[panel], other_fs)

    def in_order(body):
        if fine:
            def step(j, _):
                body(panel_of(0, j))
                body(panel_of(1, j))
                return 0
            lax.fori_loop(0, n_rep, step, 0)
        else:
            def step(j, _):
                body(j)
                return 0
            lax.fori_loop(0, panels, step, 0)

    cot_move = remote(cot_ref, cg.at[mine_t, :], tp_s.at[0], tp_r.at[0], other_tp)
    x_move = remote(x_ref, xg.at[mine_t, :], tp_s.at[1], tp_r.at[1], other_tp)
    cot_move.start()
    in_order(lambda panel: pre_copy(panel).start())
    load_x.wait()
    x_move.start()
    cg[mine_t, :] = cot_ref[...]
    xg[mine_t, :] = x_ref[...]

    def square_of(block):
        positive = jnp.maximum(block.astype(F32), 0.0)
        return (positive * positive).astype(BF16)

    def own_square(j, _):
        sq[mine_f, lanes(j)] = square_of(pre_ref[:, lanes(j)])
        return 0
    lax.fori_loop(0, panels, own_square, 0)

    def pre_arrived(panel):
        pre_copy(panel).wait_recv()
        sq[his_f, lanes(panel)] = square_of(pre_in[:, lanes(panel)])

    def gp_arrived(panel):
        gp_copy(panel).wait_recv()

    def prepare(body, j):
        if fine:
            body(panel_of(0, j))
            body(panel_of(1, j))

    def where(d, chunk, sub):
        block = (d * n_rep + chunk) * subs + sub
        return lanes(block // per_panel), pl.ds(
            pl.multiple_of(lax.rem(block, per_panel) * w, w), w)

    def down_at(d, chunk, sub):
        hid, wid = where(d, chunk, sub)
        return down_ref.at[hid, wid]

    def up_at(d, chunk, sub):
        hid, wid = where(d, chunk, sub)
        return up_ref.at[wid, hid]

    def down_block(d, chunk, sub):
        hid, wid = where(d, chunk, sub)
        return rows_dot(sq[:, hid], cg[:, wid])

    def up_block(d, chunk, sub):
        hid, wid = where(d, chunk, sub)
        return rows_dot(xg[:, wid], gp[:, hid])

    def rs_copy(first, slots, s_sem, r_sem, d, sub, s, src=None):
        src = slots.at[d, sub, s - 1] if src is None else src
        return remote(src, slots.at[d, sub, s], s_sem.at[d, sub, s], r_sem.at[d, sub, s],
                      goal[d])

    def ag_copy(at, s_sem, r_sem, d, sub, s):
        chunk = lax.rem(pos + (-s if d == 0 else s) + n_rep, n_rep)
        return remote(at(d, chunk, sub), at(d, chunk, sub), s_sem.at[d, sub, s],
                      r_sem.at[d, sub, s], goal[d])

    streams = [(d, sub) for sub in range(subs) for d in range(2)]

    def rs_open(block, first, slots, s_sem, r_sem):
        for d, sub in streams:
            first[d, sub] = block(d, chunk_of(d, 0), sub).astype(BF16)
            rs_copy(first, slots, s_sem, r_sem, d, sub, 0, first.at[d, sub]).start()

    def rs_step(block, first, slots, s_sem, r_sem, j, d, sub):
        part = block(d, chunk_of(d, j), sub)
        rs_copy(first, slots, s_sem, r_sem, d, sub, j - 1, first.at[d, sub]).wait_recv()
        slots[d, sub, j - 1] = (slots[d, sub, j - 1].astype(F32) + part).astype(BF16)
        rs_copy(first, slots, s_sem, r_sem, d, sub, j).start()

    def rs_close(block, at, first, slots, s_sem, r_sem, as_, ar, d, sub):
        part = block(d, pos, sub)
        last = n_rep - 2
        rs_copy(first, slots, s_sem, r_sem, d, sub, last, first.at[d, sub]).wait_recv()
        at(d, pos, sub)[...] = (slots[d, sub, last].astype(F32) + part).astype(BF16)
        ag_copy(at, as_, ar, d, sub, 0).start()

    def ag_step(at, as_, ar, s, d, sub):
        chunk = lax.rem(pos + (-s if d == 0 else s) + n_rep, n_rep)
        remote(at(d, chunk, sub), at(d, chunk, sub), as_.at[d, sub, s - 1],
               ar.at[d, sub, s - 1], goal[d]).wait_recv()
        ag_copy(at, as_, ar, d, sub, s).start()

    def ag_close(at, as_, ar, d, sub):
        s = n_rep - 1
        chunk = lax.rem(pos + (-s if d == 0 else s) + n_rep, n_rep)
        remote(at(d, chunk, sub), at(d, chunk, sub), as_.at[d, sub, s - 1],
               ar.at[d, sub, s - 1], goal[d]).wait_recv()

    down = (first_d, rs_d, rsd_s, rsd_r)
    up = (first_u, rs_u, rsu_s, rsu_r)

    cot_move.wait_recv()
    if fine:
        prepare(pre_arrived, 0)
    else:
        in_order(pre_arrived)
    rs_open(down_block, *down)

    load_wd.wait()
    piece = min(2 * LANES, hidden)

    def act_step(n, _):
        at = pl.ds(pl.multiple_of(n * piece, piece), piece)
        pa_out[:, at] = cols_dot(cg[his_f, :], wd[at, :]).astype(BF16)
        return 0
    lax.fori_loop(0, hidden // piece, act_step, 0)
    pa_move = remote(pa_out, pa_in, pa_s, pa_r, other_fs)
    pa_move.start()

    def act_own(n, _):
        at = pl.ds(pl.multiple_of(n * piece, piece), piece)
        pa_own[:, at] = cols_dot(cg[mine_f, :], wd[at, :])
        return 0
    lax.fori_loop(0, hidden // piece, act_own, 0)

    def down_step(j, _):
        prepare(pre_arrived, j)
        for d, sub in streams:
            rs_step(down_block, *down, j, d, sub)
        return 0
    lax.fori_loop(1, n_rep - 1, down_step, 0)
    prepare(pre_arrived, n_rep - 1)
    for d, sub in streams:
        rs_close(down_block, down_at, *down, agd_s, agd_r, d, sub)

    pa_move.wait_recv()

    def pre_grad(panel):
        at = lanes(panel)
        positive = jnp.maximum(pre_ref[:, at].astype(F32), 0.0)
        grad = pa_own[:, at] + pa_in[:, at].astype(F32)
        gp[mine_f, at] = (2.0 * positive * grad).astype(BF16)
        gp_copy(panel).start()
    in_order(pre_grad)
    x_move.wait_recv()
    for d, sub in streams:
        ag_step(down_at, agd_s, agd_r, 1, d, sub)
    if fine:
        prepare(gp_arrived, 0)
    else:
        in_order(gp_arrived)
    rs_open(up_block, *up)

    def both_step(j, _):
        prepare(gp_arrived, j)
        for d, sub in streams:
            ag_step(down_at, agd_s, agd_r, j + 1, d, sub)
            rs_step(up_block, *up, j, d, sub)
        return 0
    lax.fori_loop(1, n_rep - 2, both_step, 0)
    prepare(gp_arrived, n_rep - 2)
    for d, sub in streams:
        rs_step(up_block, *up, n_rep - 2, d, sub)
    prepare(gp_arrived, n_rep - 1)
    for d, sub in streams:
        ag_close(down_at, agd_s, agd_r, d, sub)
        rs_close(up_block, up_at, *up, agu_s, agu_r, d, sub)

    load_wu.wait()
    wide = min(2 * LANES, width)

    def input_out(n, _):
        at = pl.ds(pl.multiple_of(n * wide, wide), wide)
        gi_out[:, at] = cols_dot(gp[his_t, :], wu[at, :]).astype(BF16)
        return 0
    lax.fori_loop(0, width // wide, input_out, 0)
    gi_move = remote(gi_out, gi_in, gi_s, gi_r, other_tp)
    gi_move.start()

    def gather_step(j, _):
        for d, sub in streams:
            ag_step(up_at, agu_s, agu_r, j, d, sub)
        return 0
    lax.fori_loop(1, n_rep - 1, gather_step, 0)

    gi_move.wait_recv()

    def input_own(n, _):
        at = pl.ds(pl.multiple_of(n * wide, wide), wide)
        own = cols_dot(gp[mine_t, :], wu[at, :]).astype(BF16).astype(F32)
        gi_ref[:, at] = (own + gi_in[:, at].astype(F32)).astype(BF16)
        return 0
    lax.fori_loop(0, width // wide, input_own, 0)
    for d, sub in streams:
        ag_close(up_at, agu_s, agu_r, d, sub)

    for move in (cot_move, x_move, pa_move, gi_move):
        move.wait_send()

    def sent_panels(j, _):
        pre_copy(j).wait_send()
        gp_copy(j).wait_send()
        return 0
    lax.fori_loop(0, panels, sent_panels, 0)

    def sent_steps(s, _):
        for d, sub in streams:
            rs_copy(*down, d, sub, s, first_d.at[d, sub]).wait_send()
            rs_copy(*up, d, sub, s, first_u.at[d, sub]).wait_send()
            ag_copy(down_at, agd_s, agd_r, d, sub, s).wait_send()
            ag_copy(up_at, agu_s, agu_r, d, sub, s).wait_send()
        return 0
    lax.fori_loop(0, n_rep - 1, sent_steps, 0)


def scale_kernel(factor, pieces, gi, up, down, gi_out, up_out, down_out, up_wide, down_wide,
                 sems, gi_sem):
    copies = [pltpu.make_async_copy(gi, gi_out, gi_sem)]
    copies[0].start()
    for i in range(pieces):
        for n, (src, wide, dst) in enumerate(((up, up_wide, up_out), (down, down_wide, down_out))):
            rows = pl.ds(i * (src.shape[0] // pieces), src.shape[0] // pieces)
            wide[rows, :] = src[rows, :].astype(F32) * factor
            copy = pltpu.make_async_copy(wide.at[rows, :], dst.at[rows, :], sems.at[n, i])
            copy.start()
            copies.append(copy)
    for copy in copies:
        copy.wait()


def per_device(n_rep, inputs, pre_act, cotangent, up_weight, down_weight):
    half, width = inputs.shape
    hidden = pre_act.shape[1]
    panels = hidden // LANES
    subs, per_panel, w = plan(n_rep, width, hidden)
    dma = pltpu.SemaphoreType.DMA
    ring = [dma((2, subs, n_rep - 1))] * 2
    vmem = pl.BlockSpec(memory_space=pltpu.VMEM)
    anywhere = pl.BlockSpec(memory_space=pl.ANY)
    grad_inputs, grad_up, grad_down = pl.pallas_call(
        functools.partial(kernel, n_rep),
        name="ffn_backward",
        out_shape=(
            pltpu.VMEM((half, width), BF16),
            pltpu.VMEM((width, hidden), BF16),
            pltpu.VMEM((hidden, width), BF16),
        ),
        in_specs=[anywhere] * 5,
        out_specs=(vmem, vmem, vmem),
        scratch_shapes=[
            pltpu.VMEM((half, width), BF16),
            pltpu.VMEM((half, hidden), BF16),
            pltpu.VMEM((half, width), BF16),
            pltpu.VMEM((width, hidden), BF16),
            pltpu.VMEM((hidden, width), BF16),
            pltpu.VMEM((2 * half, width), BF16),
            pltpu.VMEM((2 * half, width), BF16),
            pltpu.VMEM((half, hidden), BF16),
            pltpu.VMEM((2 * half, hidden), BF16),
            pltpu.VMEM((2 * half, hidden), BF16),
            pltpu.VMEM((half, hidden), F32),
            pltpu.VMEM((half, hidden), BF16),
            pltpu.VMEM((half, hidden), BF16),
            pltpu.VMEM((half, width), BF16),
            pltpu.VMEM((half, width), BF16),
            pltpu.VMEM((2, subs, LANES, w), BF16),
            pltpu.VMEM((2, subs, w, LANES), BF16),
            pltpu.VMEM((2, subs, n_rep - 1, LANES, w), BF16),
            pltpu.VMEM((2, subs, n_rep - 1, w, LANES), BF16),
            dma((5,)), dma((2,)), dma((2,)),
            dma((panels,)), dma((panels,)), dma((panels,)), dma((panels,)),
            dma, dma, dma, dma,
            *ring, *ring, *ring, *ring,
        ],
        compiler_params=pltpu.CompilerParams(
            collective_id=0, has_side_effects=True, vmem_limit_bytes=50 * 2**20
        ),
    )(inputs, pre_act, cotangent, up_weight, down_weight)
    factor = (half * n_rep * lax.axis_size("tp")) ** (-0.5)
    pieces = 8
    return pl.pallas_call(
        functools.partial(scale_kernel, factor, pieces),
        name="scale_outputs",
        out_shape=(
            jax.ShapeDtypeStruct((half, width), BF16),
            jax.ShapeDtypeStruct((width, hidden), F32),
            jax.ShapeDtypeStruct((hidden, width), F32),
        ),
        in_specs=[vmem] * 3,
        out_specs=[anywhere] * 3,
        scratch_shapes=[
            pltpu.VMEM((width, hidden), F32),
            pltpu.VMEM((hidden, width), F32),
            dma((2, pieces)),
            dma,
        ],
        compiler_params=pltpu.CompilerParams(vmem_limit_bytes=40 * 2**20),
    )(*[pltpu.with_memory_space_constraint(g, pltpu.VMEM)
        for g in (grad_inputs, grad_up, grad_down)])


def solution(mesh):
    assert mesh.shape["fs"] == 2 and mesh.shape["tp"] == 2
    placed = (
        P(("rep", "tp"), "fs"),
        P(("rep", "fs"), "tp"),
        P(("rep", "tp"), "fs"),
        P("fs", "tp"),
        P("tp", "fs"),
    )
    return jax.shard_map(
        functools.partial(per_device, mesh.shape["rep"]),
        mesh=mesh,
        in_specs=placed,
        out_specs=(P(("rep", "tp"), "fs"), P("fs", "tp"), P("tp", "fs")),
        check_vma=False,
    )
```

profile of v0, /device:TPU:0, one launch (start us, length us, event | category | flops | bytes accessed | tf_op | source)
XLA Modules:
  0.0 179.8 jit_solution(15156822450796210993)
XLA Ops:
  0.6 172.9 %ffn_backward.1 = (bf16[256,1024]{1,0:T(8,128)(2,1)S(1)}, bf16[1024,2048]{1,0:T(8,128)(2,1)S(1)}, bf16[2048,1024]{1,0:T(8,128)(2,1)S(1)}) custom-call(bf16[256,1024]{1,0:T(8,128)(2,1)} %x_hbm.1, bf16[256,2048]{1,0:T(8,128)(2,1)} %pre_hbm.1, bf16[256,1024]{1,0:T(8,128)(2,1)} %cot_hbm.1, bf16[1024,2048]{1,0:T(8,128)(2,1)} %wu_hbm.1, bf16[2048,1024]{1,0:T(8,128)(2,1)} %wd_hbm.1), custom_call_target="tpu_custom_call" | custom-call | tf_op jit(solution)/shard_map/ffn_backward/pallas_call | solution.py:342
  173.6 6.2 %scale_outputs.1 = (bf16[256,1024]{1,0:T(8,128)(2,1)}, f32[1024,2048]{1,0:T(8,128)}, f32[2048,1024]{1,0:T(8,128)}) custom-call(bf16[256,1024]{1,0:T(8,128)(2,1)S(1)} %get-tuple-element.6.gi, bf16[1024,2048]{1,0:T(8,128)(2,1)S(1)} %get-tuple-element.7.up, bf16[2048,1024]{1,0:T(8,128)(2,1)S(1)} %get-tuple-element.8.down), custom_call_target="tpu_custom_call" | custom-call | tf_op jit(solution)/shard_map/scale_outputs/pallas_call | solution.py:383
where the time goes:
time: 180 us
  Pallas kernels  179 us (99%)
    pallas_call x1, Pallas kernels, per_device(): pl.pallas_call(functools.partial(kernel, n_rep), name='ffn_backward', out...  173 us
    pallas_call x1, Pallas kernels, per_device(): pl.pallas_call(functools.partial(scale_kernel, factor, pieces), name='sca...  6.2 us

commit v1 on v0

v1 whole, which is shorter than its diff:
```python
import functools

import jax
import jax.numpy as jnp
from jax import lax
from jax.experimental import pallas as pl
from jax.experimental.pallas import tpu as pltpu
from jax.sharding import PartitionSpec as P

MESH = pl.DeviceIdType.MESH
LANES = 128
F32, BF16 = jnp.float32, jnp.bfloat16

ACT, GRAD, HOP, CROSS, SPREAD, TAKE = 4, 2, 1, 1, 3, 8


def rows_dot(left, right):
    return lax.dot_general(left, right, (((0,), (0,)), ((), ())), preferred_element_type=F32)


def cols_dot(left, right):
    return lax.dot_general(left, right, (((1,), (1,)), ((), ())), preferred_element_type=F32)


def kernel(
    n_rep, x_hbm, pre_hbm, cot_hbm, wu_hbm, wd_hbm,
    gi_ref, up_ref, res,
    pre_ref, wu, wd, tok, hid, pa_own, pa_out, pa_in, gi_out, gi_in, part, out, inc,
    w_sem, tp_s, tp_r, yt_s, yt_r, ya_s, ya_r, ox_s, ox_r, fx_s, fx_r, gx_s, gx_r,
    pa_s, pa_r, gi_s, gi_r, rs_s, rs_r, fc_s, fo_s, fz_r, fy_s, fy_r,
):
    half, hidden = pre_ref.shape
    width = wd.shape[1]
    panels = hidden // LANES
    sub = LANES // 2
    rep, fs, tp = lax.axis_index("rep"), lax.axis_index("fs"), lax.axis_index("tp")
    rows_n = n_rep // 2
    mid = rows_n // 2
    row, col = rep // 2, rep % 2
    side = jnp.where(row >= mid, 1, 0)
    depth = jnp.where(row >= mid, row - mid, mid - 1 - row)
    has_outer = depth < mid - 1
    middle = depth == 0
    step = 2 * side - 1

    def rep_at(r):
        return 2 * lax.rem(r + rows_n, rows_n) + col

    outer, inner = {"rep": rep_at(row + step)}, {"rep": rep_at(row - step)}
    other_y = {"rep": 2 * row + 1 - col}
    other_fs, other_tp = {"fs": 1 - fs}, {"tp": 1 - tp}

    def block(c, b):
        return pl.ds(pl.multiple_of((2 * c + b) * half, half), half)

    own_f, own_hf = block(col, fs), block(col, 1 - fs)
    far_f, far_hf = block(1 - col, fs), block(1 - col, 1 - fs)
    own_t, own_ht = block(col, tp), block(col, 1 - tp)
    far_t, far_ht = block(1 - col, tp), block(1 - col, 1 - tp)

    def remote(src, dst, s, r, dev):
        return pltpu.make_async_remote_copy(
            src_ref=src, dst_ref=dst, send_sem=s, recv_sem=r, device_id=dev,
            device_id_type=MESH)

    barrier = pltpu.get_barrier_semaphore()
    for dev in (outer, inner, other_y, other_fs, other_tp):
        pl.semaphore_signal(barrier, inc=1, device_id=dev, device_id_type=MESH)
    held = ((cot_hbm, tok.at[1, own_t]), (x_hbm, tok.at[0, own_t]), (pre_hbm, pre_ref),
            (wd_hbm, wd), (wu_hbm, wu))
    loads = [pltpu.make_async_copy(src, dst, w_sem.at[i]) for i, (src, dst) in enumerate(held)]
    load_cot, load_x, load_pre, load_wd, load_wu = loads
    for load in loads:
        load.start()
    load_cot.wait()
    load_x.wait()
    pl.semaphore_wait(barrier, 5)

    def lanes(k):
        return pl.ds(pl.multiple_of(k * LANES, LANES), LANES)

    def rows(k, s):
        return pl.ds(pl.multiple_of(k * LANES + s * sub, sub), sub)

    def moved(ref, at, s, r, dev):
        return remote(ref.at[at], ref.at[at], s, r, dev)

    y_move = moved(tok, (1 - col, own_t), yt_s, yt_r, other_y)
    y_move.start()
    cot_move = moved(tok, (1, own_t), tp_s.at[0], tp_r.at[0], other_tp)
    cot_move.start()
    x_move = moved(tok, (0, own_t), tp_s.at[1], tp_r.at[1], other_tp)
    far_move = moved(tok, (col, far_t), tp_s.at[2], tp_r.at[2], other_tp)

    @pl.when(col == 0)
    def _():
        x_move.start()

    def ya_copy(k):
        return moved(hid, (1 - col, own_f, lanes(k)), ya_s.at[k], ya_r.at[k], other_y)

    def ox_copy(k):
        return moved(hid, (col, own_f, lanes(k)), ox_s.at[k], ox_r.at[k], other_fs)

    def fx_copy(k):
        return moved(hid, (col, far_f, lanes(k)), fx_s.at[k], fx_r.at[k], other_fs)

    def gx_copy(k):
        return moved(hid, (0, own_f, lanes(k)), gx_s.at[k], gx_r.at[k], other_fs)

    def pa_copy(k):
        return remote(pa_out.at[:, lanes(k)], pa_in.at[:, lanes(k)], pa_s.at[k], pa_r.at[k],
                      other_fs)

    load_pre.wait()

    def own_square(k, _):
        positive = jnp.maximum(pre_ref[:, lanes(k)].astype(F32), 0.0)
        hid[1, own_f, lanes(k)] = (positive * positive).astype(BF16)

        @pl.when(col == 0)
        def _():
            ya_copy(k).start()
        return 0
    lax.fori_loop(0, panels, own_square, 0)
    load_wd.wait()
    cot_move.wait_recv()

    def act(k):
        pa_out[:, lanes(k)] = cols_dot(tok[1, own_hf, :], wd[lanes(k), :]).astype(BF16)
        pa_copy(k).start()

        @pl.when(col == 1)
        def _():
            ox_copy(k).start()
        pa_own[:, lanes(k)] = cols_dot(tok[1, own_f, :], wd[lanes(k), :])

    def grad(k):
        pa_copy(k).wait_recv()
        positive = jnp.maximum(pre_ref[:, lanes(k)].astype(F32), 0.0)
        total = pa_own[:, lanes(k)] + pa_in[:, lanes(k)].astype(F32)
        hid[0, own_f, lanes(k)] = (2.0 * positive * total).astype(BF16)

        @pl.when(col == 0)
        def _():
            ox_copy(k).start()

        @pl.when(col == 1)
        def _():
            ya_copy(k).start()

    def hop(k):
        remote(hid.at[1 - col, own_f, lanes(k)], hid.at[col, far_f, lanes(k)], ya_s.at[k],
               ya_r.at[k], other_y).wait_recv()
        fx_copy(k).start()

    def rs_copy(k, s):
        slot = jnp.where(middle, 1, 0)
        return remote(out.at[rows(k, s)], inc.at[slot, rows(k, s)], rs_s.at[k, s],
                      rs_r.at[slot, k, s], inner)

    def rs_wait(slot, k, s):
        remote(out.at[rows(k, s)], inc.at[slot, rows(k, s)], rs_s.at[k, s],
               rs_r.at[slot, k, s], inner).wait_recv()

    def final(k, s, sem, dev):
        return moved(res, (col, rows(k, s)), sem, fz_r.at[k, s], dev)

    def final_y(k, s):
        return moved(res, (col, rows(k, s)), fy_s.at[k, s], fy_r.at[k, s], other_y)

    def reduce(k):
        ox_copy(k).wait_recv()
        fx_copy(k).wait_recv()
        part[...] = rows_dot(hid[col, :, lanes(k)], tok[col])
        for s in (1 - side, side):
            mine = part[pl.ds(pl.multiple_of(s * sub, sub), sub), :]

            @pl.when(has_outer)
            def _():
                rs_wait(0, k, s)
                out[rows(k, s), :] = (mine + inc[0, rows(k, s), :].astype(F32)).astype(BF16)

            @pl.when(jnp.logical_not(has_outer))
            def _():
                out[rows(k, s), :] = mine.astype(BF16)

            if s is side:
                @pl.when(jnp.logical_not(middle))
                def _():
                    rs_copy(k, s).start()
            else:
                rs_copy(k, s).start()

    def spread(k, s):
        @pl.when(has_outer)
        def _():
            final(k, s, fo_s.at[k, s], outer).start()
        final_y(k, s).start()

    def cross(k):
        @pl.when(middle)
        def _():
            at = rows(k, side)
            rs_wait(1, k, side)
            res[col, at, :] = (out[at, :].astype(F32) + inc[1, at, :].astype(F32)).astype(BF16)
            final(k, side, fc_s.at[k], inner).start()
            spread(k, side)

    def forward(k):
        final(k, 1 - side, fc_s.at[k], inner).wait_recv()
        spread(k, 1 - side)

        @pl.when(jnp.logical_not(middle))
        def _():
            final(k, side, fc_s.at[k], inner).wait_recv()
            spread(k, side)

    def take(k):
        for s in range(2):
            moved(res, (1 - col, rows(k, s)), fy_s.at[k, s], fy_r.at[k, s], other_y).wait_recv()
        up_ref[:, lanes(k)] = res[0, lanes(k), :].T

    def early(k, _):
        act(k)
        return 0
    lax.fori_loop(0, ACT, early, 0)

    def early_grad(k, _):
        grad(k)
        return 0
    lax.fori_loop(0, GRAD, early_grad, 0)
    remote(tok.at[1 - col, own_t], tok.at[col, far_t], yt_s, yt_r, other_y).wait_recv()
    far_move.start()

    @pl.when(col == 0)
    def _():
        x_move.wait_recv()

    def early_hop(k, _):
        hop(k)
        return 0
    lax.fori_loop(0, HOP, early_hop, 0)
    far_move.wait_recv()

    def main(i, _):
        @pl.when(i + ACT < panels)
        def _():
            act(i + ACT)

        @pl.when(i + GRAD < panels)
        def _():
            grad(i + GRAD)

        @pl.when(i + HOP < panels)
        def _():
            hop(i + HOP)
        reduce(i)

        @pl.when(i >= CROSS)
        def _():
            cross(i - CROSS)

        @pl.when(i >= SPREAD)
        def _():
            forward(i - SPREAD)

        @pl.when((col == 1) & (i >= panels // 2))
        def _():
            for n in range(2):
                gx_copy(2 * (i - panels // 2) + n).start()

        @pl.when(i >= TAKE)
        def _():
            take(i - TAKE)
        return 0
    lax.fori_loop(0, panels, main, 0)
    load_wu.wait()
    cross(panels - 1)
    forward(panels - 3)

    @pl.when(col == 1)
    def _():
        def gx_wait(k, _):
            gx_copy(k).wait_recv()
            return 0
        lax.fori_loop(0, panels, gx_wait, 0)

    wide = min(2 * LANES, width)

    def input_out(n, _):
        at = pl.ds(pl.multiple_of(n * wide, wide), wide)
        gi_out[:, at] = cols_dot(hid[0, own_ht, :], wu[at, :]).astype(BF16)
        return 0
    lax.fori_loop(0, width // wide, input_out, 0)
    gi_move = remote(gi_out, gi_in, gi_s, gi_r, other_tp)
    gi_move.start()
    forward(panels - 2)

    def late(k, _):
        take(k)
        return 0
    lax.fori_loop(panels - TAKE, panels - 5, late, 0)
    forward(panels - 1)

    def input_own(n, _):
        at = pl.ds(pl.multiple_of(n * wide, wide), wide)
        mine = cols_dot(hid[0, own_t, :], wu[at, :]).astype(BF16).astype(F32)
        gi_ref[:, at] = mine.astype(BF16)
        return 0
    lax.fori_loop(0, width // wide, input_own, 0)
    gi_move.wait_recv()
    gi_ref[...] = (gi_ref[...].astype(F32) + gi_in[...].astype(F32)).astype(BF16)
    lax.fori_loop(panels - 5, panels, late, 0)

    for move in (y_move, cot_move, far_move, gi_move):
        move.wait_send()

    @pl.when(col == 0)
    def _():
        x_move.wait_send()

    def sent(k, _):
        for copy in (pa_copy, ya_copy, ox_copy, fx_copy):
            copy(k).wait_send()

        @pl.when(col == 1)
        def _():
            gx_copy(k).wait_send()

        rs_copy(k, 1 - side).wait_send()

        @pl.when(middle)
        def _():
            final(k, side, fc_s.at[k], inner).wait_send()

        @pl.when(jnp.logical_not(middle))
        def _():
            rs_copy(k, side).wait_send()
        for s in range(2):
            final_y(k, s).wait_send()

            @pl.when(has_outer)
            def _():
                final(k, s, fo_s.at[k, s], outer).wait_send()
        return 0
    lax.fori_loop(0, panels, sent, 0)


def scale_kernel(factor, pieces, gi, up, res, gi_out, up_out, down_out, up_wide, down_wide,
                 sems, gi_sem):
    copies = [pltpu.make_async_copy(gi, gi_out, gi_sem)]
    copies[0].start()
    for i in range(pieces):
        for n, (src, wide, dst) in enumerate(
                ((up, up_wide, up_out), (res.at[1], down_wide, down_out))):
            rows = pl.ds(i * (src.shape[0] // pieces), src.shape[0] // pieces)
            wide[rows, :] = src[rows, :].astype(F32) * factor
            copy = pltpu.make_async_copy(wide.at[rows, :], dst.at[rows, :], sems.at[n, i])
            copy.start()
            copies.append(copy)
    for copy in copies:
        copy.wait()


def per_device(n_rep, inputs, pre_act, cotangent, up_weight, down_weight):
    half, width = inputs.shape
    hidden = pre_act.shape[1]
    panels = hidden // LANES
    dma = pltpu.SemaphoreType.DMA
    vmem = pl.BlockSpec(memory_space=pltpu.VMEM)
    anywhere = pl.BlockSpec(memory_space=pl.ANY)
    one, two = dma((panels,)), dma((panels, 2))
    grad_inputs, grad_up, result = pl.pallas_call(
        functools.partial(kernel, n_rep),
        name="ffn_backward",
        out_shape=(
            pltpu.VMEM((half, width), BF16),
            pltpu.VMEM((width, hidden), BF16),
            pltpu.VMEM((2, hidden, width), BF16),
        ),
        in_specs=[anywhere] * 5,
        out_specs=(vmem, vmem, vmem),
        scratch_shapes=[
            pltpu.VMEM((half, hidden), BF16),
            pltpu.VMEM((width, hidden), BF16),
            pltpu.VMEM((hidden, width), BF16),
            pltpu.VMEM((2, 4 * half, width), BF16),
            pltpu.VMEM((2, 4 * half, hidden), BF16),
            pltpu.VMEM((half, hidden), F32),
            pltpu.VMEM((half, hidden), BF16),
            pltpu.VMEM((half, hidden), BF16),
            pltpu.VMEM((half, width), BF16),
            pltpu.VMEM((half, width), BF16),
            pltpu.VMEM((LANES, width), F32),
            pltpu.VMEM((hidden, width), BF16),
            pltpu.VMEM((2, hidden, width), BF16),
            dma((5,)), dma((3,)), dma((3,)), dma, dma,
            one, one, one, one, one, one, one, one,
            one, one, dma, dma,
            two, dma((2, panels, 2)), one, two, two, two, two,
        ],
        compiler_params=pltpu.CompilerParams(
            collective_id=0, has_side_effects=True, vmem_limit_bytes=48 * 2**20
        ),
    )(inputs, pre_act, cotangent, up_weight, down_weight)
    factor = (half * n_rep * lax.axis_size("tp")) ** (-0.5)
    pieces = 8
    return pl.pallas_call(
        functools.partial(scale_kernel, factor, pieces),
        name="scale_outputs",
        out_shape=(
            jax.ShapeDtypeStruct((half, width), BF16),
            jax.ShapeDtypeStruct((width, hidden), F32),
            jax.ShapeDtypeStruct((hidden, width), F32),
        ),
        in_specs=[vmem] * 3,
        out_specs=[anywhere] * 3,
        scratch_shapes=[
            pltpu.VMEM((width, hidden), F32),
            pltpu.VMEM((hidden, width), F32),
            dma((2, pieces)),
            dma,
        ],
        compiler_params=pltpu.CompilerParams(vmem_limit_bytes=40 * 2**20),
    )(*[pltpu.with_memory_space_constraint(g, pltpu.VMEM)
        for g in (grad_inputs, grad_up, result)])


def solution(mesh):
    assert mesh.shape["fs"] == 2 and mesh.shape["tp"] == 2 and mesh.shape["rep"] % 4 == 0
    placed = (
        P(("rep", "tp"), "fs"),
        P(("rep", "fs"), "tp"),
        P(("rep", "tp"), "fs"),
        P("fs", "tp"),
        P("tp", "fs"),
    )
    return jax.shard_map(
        functools.partial(per_device, mesh.shape["rep"]),
        mesh=mesh,
        in_specs=placed,
        out_specs=(P(("rep", "tp"), "fs"), P("fs", "tp"), P("tp", "fs")),
        check_vma=False,
    )
```

time: 180 us -> 236 us (1.31)
  Pallas kernels: 179 us -> 234 us
    pallas_call x1, Pallas kernels: 173 us -> 228 us  [per_device(): pl.pallas_call(functools.partial(kernel, n_rep), name='ffn_backward', out...]
where the time goes in v1:
time: 236 us; the launch traced here: 235 us
  Pallas kernels  234 us (99%)
    pallas_call x1, Pallas kernels, per_device(): pl.pallas_call(functools.partial(kernel, n_rep), name='ffn_backward', out...  228 us
    pallas_call x1, Pallas kernels, per_device(): pl.pallas_call(functools.partial(scale_kernel, factor, pieces), name='sca...  6.2 us

profile of v1, /device:TPU:0, one launch (start us, length us, event | category | flops | bytes accessed | tf_op | source)
XLA Modules:
  0.0 234.5 jit_solution(6900548636093263431)
XLA Ops:
  0.6 227.7 %ffn_backward.1 = (bf16[256,1024]{1,0:T(8,128)(2,1)S(1)}, bf16[1024,2048]{1,0:T(8,128)(2,1)S(1)}, bf16[2,2048,1024]{2,1,0:T(8,128)(2,1)S(1)}) custom-call(bf16[256,1024]{1,0:T(8,128)(2,1)} %x_hbm.1, bf16[256,2048]{1,0:T(8,128)(2,1)} %pre_hbm.1, bf16[256,1024]{1,0:T(8,128)(2,1)} %cot_hbm.1, bf16[1024,2048]{1,0:T(8,128)(2,1)} %wu_hbm.1, bf16[2048,1024]{1,0:T(8,128)(2,1)} %wd_hbm.1), custom_call_target="tpu_custom_call" | custom-call | tf_op jit(solution)/shard_map/ffn_backward/pallas_call | solution.py:374
  228.3 6.2 %scale_outputs.1 = (bf16[256,1024]{1,0:T(8,128)(2,1)}, f32[1024,2048]{1,0:T(8,128)}, f32[2048,1024]{1,0:T(8,128)}) custom-call(bf16[256,1024]{1,0:T(8,128)(2,1)S(1)} %get-tuple-element.6.gi, bf16[1024,2048]{1,0:T(8,128)(2,1)S(1)} %get-tuple-element.7.up, bf16[2,2048,1024]{2,1,0:T(8,128)(2,1)S(1)} %get-tuple-element.8.res), custom_call_target="tpu_custom_call" | custom-call | tf_op jit(solution)/shard_map/scale_outputs/pallas_call | solution.py:409

commit v2 on v1

v2 whole, which is shorter than its diff:
```python
import functools

import jax
import jax.numpy as jnp
from jax import lax
from jax.experimental import pallas as pl
from jax.experimental.pallas import tpu as pltpu
from jax.sharding import PartitionSpec as P

MESH = pl.DeviceIdType.MESH
LANES = 128
F32, BF16 = jnp.float32, jnp.bfloat16

FIRST, START, MORE, HOP, PACE = 4, 2, 5, 2, 3
CROSS, SPREAD, APART, TAKE = 2, 4, 4, 6


def rows_dot(left, right):
    return lax.dot_general(left, right, (((0,), (0,)), ((), ())), preferred_element_type=F32)


def cols_dot(left, right):
    return lax.dot_general(left, right, (((1,), (1,)), ((), ())), preferred_element_type=F32)


def kernel(
    n_rep, x_hbm, pre_hbm, cot_hbm, wu_hbm, wd_hbm,
    gi_ref, up_ref, res,
    pre_ref, wu, wd, tok, hid, pa_own, pa_out, pa_in, gi_out, gi_in, part, out, inc,
    w_sem, tp_s, tp_r, yt_s, yt_r, ya_s, ya_r, ox_s, fx_s, act_r, gx_s, gx_r,
    pa_s, pa_r, gi_s, gi_r, rs_s, rs_r, fc_s, fo_s, fz_r, fy_s, fy_r,
):
    half, hidden = pre_ref.shape
    width = wd.shape[1]
    panels = hidden // LANES
    sub, wide = LANES // 2, width // 2
    chunks = 2 * panels
    rep, fs, tp = lax.axis_index("rep"), lax.axis_index("fs"), lax.axis_index("tp")
    rows_n = n_rep // 2
    mid = rows_n // 2
    row, col = rep // 2, rep % 2
    side = jnp.where(row >= mid, 1, 0)
    depth = jnp.where(row >= mid, row - mid, mid - 1 - row)
    has_outer = depth < mid - 1
    middle = depth == 0
    step = 2 * side - 1

    def rep_at(r):
        return 2 * lax.rem(r + rows_n, rows_n) + col

    outer, inner = {"rep": rep_at(row + step)}, {"rep": rep_at(row - step)}
    other_y = {"rep": 2 * row + 1 - col}
    other_fs, other_tp = {"fs": 1 - fs}, {"tp": 1 - tp}

    def block(c, b):
        return pl.ds(pl.multiple_of((2 * c + b) * half, half), half)

    own_f, own_hf = block(col, fs), block(col, 1 - fs)
    far_f, far_hf = block(1 - col, fs), block(1 - col, 1 - fs)
    own_t, own_ht = block(col, tp), block(col, 1 - tp)
    far_t, far_ht = block(1 - col, tp), block(1 - col, 1 - tp)

    def remote(src, dst, s, r, dev):
        return pltpu.make_async_remote_copy(
            src_ref=src, dst_ref=dst, send_sem=s, recv_sem=r, device_id=dev,
            device_id_type=MESH)

    barrier = pltpu.get_barrier_semaphore()
    for dev in (outer, inner, other_y, other_fs, other_tp):
        pl.semaphore_signal(barrier, inc=1, device_id=dev, device_id_type=MESH)
    held = ((cot_hbm, tok.at[1, own_t]), (x_hbm, tok.at[0, own_t]), (pre_hbm, pre_ref),
            (wd_hbm, wd), (wu_hbm, wu))
    loads = [pltpu.make_async_copy(src, dst, w_sem.at[i]) for i, (src, dst) in enumerate(held)]
    load_cot, load_x, load_pre, load_wd, load_wu = loads
    for load in loads:
        load.start()
    load_cot.wait()
    load_x.wait()
    pl.semaphore_wait(barrier, 5)

    def lanes(k):
        return pl.ds(pl.multiple_of(k * LANES, LANES), LANES)

    def where_is(k):
        early = k < 4
        return jnp.where(early, k % 2, k // 2), jnp.where(early, k // 2, k % 2)

    def cols(w):
        return pl.ds(pl.multiple_of(w * wide, wide), wide)

    def piece(k, s):
        p, w = where_is(k)
        return pl.ds(pl.multiple_of(p * LANES + s * sub, sub), sub), cols(w)

    def moved(ref, at, s, r, dev):
        return remote(ref.at[at], ref.at[at], s, r, dev)

    def y_move(w):
        return moved(tok, (1 - col, own_t, cols(w)), yt_s.at[w], yt_r.at[w], other_y)

    def far_move(w):
        return moved(tok, (col, far_t, cols(w)), tp_s.at[2 + w], tp_r.at[2 + w], other_tp)

    y_move(0).start()
    cot_move = moved(tok, (1, own_t), tp_s.at[0], tp_r.at[0], other_tp)
    cot_move.start()
    x_move = moved(tok, (0, own_t), tp_s.at[1], tp_r.at[1], other_tp)

    @pl.when(col == 0)
    def _():
        x_move.start()

    def ya_copy(k):
        return moved(hid, (1 - col, own_f, lanes(k)), ya_s, ya_r.at[k], other_y)

    def ox_copy(k):
        return moved(hid, (col, own_f, lanes(k)), ox_s, act_r.at[k], other_fs)

    def fx_copy(k):
        return moved(hid, (col, far_f, lanes(k)), fx_s, act_r.at[k], other_fs)

    def gx_copy(k):
        return moved(hid, (0, own_f, lanes(k)), gx_s, gx_r, other_fs)

    def pa_copy(k):
        return remote(pa_out.at[:, lanes(k)], pa_in.at[:, lanes(k)], pa_s, pa_r.at[k],
                      other_fs)

    load_pre.wait()

    def each(lo, hi, body):
        def once(k, _):
            body(k)
            return 0
        lax.fori_loop(lo, hi, once, 0)

    def own_square(k):
        positive = jnp.maximum(pre_ref[:, lanes(k)].astype(F32), 0.0)
        hid[1, own_f, lanes(k)] = (positive * positive).astype(BF16)

        @pl.when(col == 0)
        def _():
            ya_copy(k).start()

    each(0, 2, own_square)

    @pl.when(col == 0)
    def _():
        y_move(1).start()
    each(2, panels, own_square)
    load_wd.wait()
    cot_move.wait_recv()

    def act(k):
        pa_out[:, lanes(k)] = cols_dot(tok[1, own_hf, :], wd[lanes(k), :]).astype(BF16)
        pa_copy(k).start()
        pa_own[:, lanes(k)] = cols_dot(tok[1, own_f, :], wd[lanes(k), :])

    def pair(k):
        ox_copy(k).start()

    def grad(k):
        pa_copy(k).wait_recv()
        positive = jnp.maximum(pre_ref[:, lanes(k)].astype(F32), 0.0)
        total = pa_own[:, lanes(k)] + pa_in[:, lanes(k)].astype(F32)
        hid[0, own_f, lanes(k)] = (2.0 * positive * total).astype(BF16)

        @pl.when(col == 1)
        def _():
            ya_copy(k).start()

    def hop(k):
        remote(hid.at[1 - col, own_f, lanes(k)], hid.at[col, far_f, lanes(k)], ya_s,
               ya_r.at[k], other_y).wait_recv()
        fx_copy(k).start()

    def rs_copy(k, s):
        slot = jnp.where(middle, 1, 0)
        return remote(out.at[piece(k, s)], inc.at[(slot, *piece(k, s))], rs_s,
                      rs_r.at[jnp.where(middle, 2, s), k], inner)

    def rs_wait(slot, k, s):
        remote(out.at[piece(k, s)], inc.at[(slot, *piece(k, s))], rs_s,
               rs_r.at[2 if slot else s, k], inner).wait_recv()

    def final(k, s, sem, dev):
        return moved(res, (col, *piece(k, s)), sem, fz_r.at[k, s], dev)

    def final_y(k, s):
        return moved(res, (col, *piece(k, s)), fy_s, fy_r.at[k], other_y)

    def arrive(k):
        moved(hid, (col, pl.ds(0, 2 * half), lanes(k)), ox_s, act_r.at[k], other_fs).wait_recv()

    def reduce(k):
        p, w = where_is(k)
        part[...] = rows_dot(hid[col, :, lanes(p)], tok[col, :, cols(w)])
        for s in (1 - side, side):
            at = piece(k, s)
            mine = part[pl.ds(pl.multiple_of(s * sub, sub), sub), :]

            @pl.when(has_outer)
            def _():
                rs_wait(0, k, s)
                out[at] = (mine + inc[(0, *at)].astype(F32)).astype(BF16)

            @pl.when(jnp.logical_not(has_outer))
            def _():
                out[at] = mine.astype(BF16)

            if s is side:
                @pl.when(jnp.logical_not(middle))
                def _():
                    rs_copy(k, s).start()
            else:
                rs_copy(k, s).start()

    def spread(k, s):
        @pl.when(has_outer)
        def _():
            final(k, s, fo_s, outer).start()
        final_y(k, s).start()

    def cross(k):
        @pl.when(middle)
        def _():
            at = piece(k, side)
            rs_wait(1, k, side)
            res[(col, *at)] = (out[at].astype(F32) + inc[(1, *at)].astype(F32)).astype(BF16)
            final(k, side, fc_s, inner).start()
            spread(k, side)

    def forward(k):
        final(k, 1 - side, fc_s, inner).wait_recv()
        spread(k, 1 - side)

        @pl.when(jnp.logical_not(middle))
        def _():
            final(k, side, fc_s, inner).wait_recv()
            spread(k, side)

    def take(k):
        p, w = where_is(k)
        at = (lanes(p), cols(w))
        moved(res, (1 - col, *at), fy_s, fy_r.at[k], other_y).wait_recv()
        up_ref[cols(w), lanes(p)] = res[(0, *at)].T

    def when_in(i, end, body):
        @pl.when((i >= 0) & (i < end))
        def _():
            body(i)

    each(0, FIRST, act)

    def ready(k):
        grad(k)
        pair(k)
    each(0, START, ready)

    @pl.when(col == 1)
    def _():
        y_move(1).start()
    act(FIRST)
    more = FIRST + 1 + MORE

    def far_arrived(w):
        remote(tok.at[1 - col, own_t, cols(w)], tok.at[col, far_t, cols(w)], yt_s.at[w],
               yt_r.at[w], other_y).wait_recv()
        far_move(w).start()

    far_arrived(0)

    @pl.when(col == 0)
    def _():
        x_move.wait_recv()

    each(0, HOP, hop)
    far_move(0).wait_recv()
    each(FIRST + 1, more, act)
    each(START, START + PACE, grad)

    furthest = SPREAD + APART * (mid - 1)
    take_lag = furthest + TAKE

    def spreading(k):
        when_in(k - CROSS, chunks, cross)
        when_in(k - SPREAD - APART * depth, chunks, forward)
        when_in(k - take_lag, chunks, take)

    def main(i):
        @pl.when(i == 1)
        def _():
            far_arrived(1)
            far_move(1).wait_recv()
        for n in range(2):
            @pl.when(i == 0)
            def _():
                arrive(n)
            if n == 0:
                @pl.when(i > 1)
                def _():
                    arrive(i)
            reduce(2 * i + n)

            if n == 0:
                for step in range(PACE):
                    when_in(more + PACE * i + step, panels, act)
                    when_in(START + PACE + PACE * i + step, panels, grad)
                when_in(i + HOP, panels, pair)
                when_in(i + HOP, panels, hop)
            spreading(2 * i + n)

        @pl.when((col == 1) & (i >= panels // 2))
        def _():
            for n in range(2):
                gx_copy(2 * (i - panels // 2) + n).start()

    each(0, panels, main)
    each(chunks, chunks + 2, spreading)
    load_wu.wait()

    @pl.when(col == 1)
    def _():
        moved(hid, (0, own_f), gx_s, gx_r, other_fs).wait_recv()

    strip = min(2 * LANES, width)

    def input_out(n):
        at = pl.ds(pl.multiple_of(n * strip, strip), strip)
        gi_out[:, at] = cols_dot(hid[0, own_ht, :], wu[at, :]).astype(BF16)
    each(0, width // strip, input_out)
    gi_move = remote(gi_out, gi_in, gi_s, gi_r, other_tp)
    gi_move.start()
    each(chunks + 2, chunks + 6, spreading)

    def input_own(n):
        at = pl.ds(pl.multiple_of(n * strip, strip), strip)
        mine = cols_dot(hid[0, own_t, :], wu[at, :]).astype(BF16).astype(F32)
        gi_ref[:, at] = mine.astype(BF16)
    each(0, width // strip, input_own)
    gi_move.wait_recv()
    gi_ref[...] = (gi_ref[...].astype(F32) + gi_in[...].astype(F32)).astype(BF16)
    each(chunks + 6, chunks + take_lag, spreading)

    for move in (y_move(0), y_move(1), cot_move, far_move(0), far_move(1), gi_move):
        move.wait_send()
    some = pl.ds(0, hidden // 2)
    remote(pa_out, pa_in, pa_s, pa_r.at[0], other_fs).wait_send()
    moved(hid, (1 - col, own_f), ya_s, ya_r.at[0], other_y).wait_send()
    moved(hid, (col, own_f), ox_s, act_r.at[0], other_fs).wait_send()
    moved(hid, (col, far_f), fx_s, act_r.at[0], other_fs).wait_send()
    moved(res, (col,), fy_s, fy_r.at[0], other_y).wait_send()

    @pl.when(col == 0)
    def _():
        x_move.wait_send()

    @pl.when(col == 1)
    def _():
        moved(hid, (0, own_f), gx_s, gx_r, other_fs).wait_send()

    @pl.when(middle)
    def _():
        remote(out.at[some], inc.at[1, some], rs_s, rs_r.at[2, 0], inner).wait_send()
        moved(res, (col, some), fc_s, fz_r.at[0, 0], inner).wait_send()

    @pl.when(jnp.logical_not(middle))
    def _():
        remote(out, inc.at[0], rs_s, rs_r.at[0, 0], inner).wait_send()

    @pl.when(has_outer)
    def _():
        moved(res, (col,), fo_s, fz_r.at[0, 0], outer).wait_send()


def scale_kernel(factor, pieces, gi, up, res, gi_out, up_out, down_out, up_wide, down_wide,
                 sems, gi_sem):
    copies = [pltpu.make_async_copy(gi, gi_out, gi_sem)]
    copies[0].start()
    for i in range(pieces):
        for n, (src, wide, dst) in enumerate(
                ((up, up_wide, up_out), (res.at[1], down_wide, down_out))):
            rows = pl.ds(i * (src.shape[0] // pieces), src.shape[0] // pieces)
            wide[rows, :] = src[rows, :].astype(F32) * factor
            copy = pltpu.make_async_copy(wide.at[rows, :], dst.at[rows, :], sems.at[n, i])
            copy.start()
            copies.append(copy)
    for copy in copies:
        copy.wait()


def per_device(n_rep, inputs, pre_act, cotangent, up_weight, down_weight):
    half, width = inputs.shape
    hidden = pre_act.shape[1]
    panels = hidden // LANES
    dma = pltpu.SemaphoreType.DMA
    vmem = pl.BlockSpec(memory_space=pltpu.VMEM)
    anywhere = pl.BlockSpec(memory_space=pl.ANY)
    chunks = 2 * panels
    one = dma((panels,))
    grad_inputs, grad_up, result = pl.pallas_call(
        functools.partial(kernel, n_rep),
        name="ffn_backward",
        out_shape=(
            pltpu.VMEM((half, width), BF16),
            pltpu.VMEM((width, hidden), BF16),
            pltpu.VMEM((2, hidden, width), BF16),
        ),
        in_specs=[anywhere] * 5,
        out_specs=(vmem, vmem, vmem),
        scratch_shapes=[
            pltpu.VMEM((half, hidden), BF16),
            pltpu.VMEM((width, hidden), BF16),
            pltpu.VMEM((hidden, width), BF16),
            pltpu.VMEM((2, 4 * half, width), BF16),
            pltpu.VMEM((2, 4 * half, hidden), BF16),
            pltpu.VMEM((half, hidden), F32),
            pltpu.VMEM((half, hidden), BF16),
            pltpu.VMEM((half, hidden), BF16),
            pltpu.VMEM((half, width), BF16),
            pltpu.VMEM((half, width), BF16),
            pltpu.VMEM((LANES, width // 2), F32),
            pltpu.VMEM((hidden, width), BF16),
            pltpu.VMEM((2, hidden, width), BF16),
            dma((5,)), dma((4,)), dma((4,)), dma((2,)), dma((2,)),
            dma, one, dma, dma, one, dma, dma,
            dma, one, dma, dma,
            dma, dma((3, chunks)), dma, dma, dma((chunks, 2)), dma, dma((chunks,)),
        ],
        compiler_params=pltpu.CompilerParams(
            collective_id=0, has_side_effects=True, vmem_limit_bytes=48 * 2**20
        ),
    )(inputs, pre_act, cotangent, up_weight, down_weight)
    factor = (half * n_rep * lax.axis_size("tp")) ** (-0.5)
    pieces = 8
    return pl.pallas_call(
        functools.partial(scale_kernel, factor, pieces),
        name="scale_outputs",
        out_shape=(
            jax.ShapeDtypeStruct((half, width), BF16),
            jax.ShapeDtypeStruct((width, hidden), F32),
            jax.ShapeDtypeStruct((hidden, width), F32),
        ),
        in_specs=[vmem] * 3,
        out_specs=[anywhere] * 3,
        scratch_shapes=[
            pltpu.VMEM((width, hidden), F32),
            pltpu.VMEM((hidden, width), F32),
            dma((2, pieces)),
            dma,
        ],
        compiler_params=pltpu.CompilerParams(vmem_limit_bytes=40 * 2**20),
    )(*[pltpu.with_memory_space_constraint(g, pltpu.VMEM)
        for g in (grad_inputs, grad_up, result)])


def solution(mesh):
    assert mesh.shape["fs"] == 2 and mesh.shape["tp"] == 2 and mesh.shape["rep"] % 4 == 0
    placed = (
        P(("rep", "tp"), "fs"),
        P(("rep", "fs"), "tp"),
        P(("rep", "tp"), "fs"),
        P("fs", "tp"),
        P("tp", "fs"),
    )
    return jax.shard_map(
        functools.partial(per_device, mesh.shape["rep"]),
        mesh=mesh,
        in_specs=placed,
        out_specs=(P(("rep", "tp"), "fs"), P("fs", "tp"), P("tp", "fs")),
        check_vma=False,
    )
```

time: 236 us -> 150 us (0.64)
  Pallas kernels: 234 us -> 149 us
    pallas_call x1, Pallas kernels: 228 us -> 143 us  [per_device(): pl.pallas_call(functools.partial(kernel, n_rep), name='ffn_backward', out...]
where the time goes in v2:
time: 150 us; the launch traced here: 149 us
  Pallas kernels  149 us (99%)
    pallas_call x1, Pallas kernels, per_device(): pl.pallas_call(functools.partial(kernel, n_rep), name='ffn_backward', out...  143 us
    pallas_call x1, Pallas kernels, per_device(): pl.pallas_call(functools.partial(scale_kernel, factor, pieces), name='sca...  6.2 us

profile of v2, /device:TPU:0, one launch (start us, length us, event | category | flops | bytes accessed | tf_op | source)
XLA Modules:
  0.0 149.4 jit_solution(12411179726494389784)
XLA Ops:
  0.6 142.5 %ffn_backward.1 = (bf16[256,1024]{1,0:T(8,128)(2,1)S(1)}, bf16[1024,2048]{1,0:T(8,128)(2,1)S(1)}, bf16[2,2048,1024]{2,1,0:T(8,128)(2,1)S(1)}) custom-call(bf16[256,1024]{1,0:T(8,128)(2,1)} %x_hbm.1, bf16[256,2048]{1,0:T(8,128)(2,1)} %pre_hbm.1, bf16[256,1024]{1,0:T(8,128)(2,1)} %cot_hbm.1, bf16[1024,2048]{1,0:T(8,128)(2,1)} %wu_hbm.1, bf16[2048,1024]{1,0:T(8,128)(2,1)} %wd_hbm.1), custom_call_target="tpu_custom_call" | custom-call | tf_op jit(solution)/shard_map/ffn_backward/pallas_call | solution.py:401
  143.2 6.2 %scale_outputs.1 = (bf16[256,1024]{1,0:T(8,128)(2,1)}, f32[1024,2048]{1,0:T(8,128)}, f32[2048,1024]{1,0:T(8,128)}) custom-call(bf16[256,1024]{1,0:T(8,128)(2,1)S(1)} %get-tuple-element.6.gi, bf16[1024,2048]{1,0:T(8,128)(2,1)S(1)} %get-tuple-element.7.up, bf16[2,2048,1024]{2,1,0:T(8,128)(2,1)S(1)} %get-tuple-element.8.res), custom_call_target="tpu_custom_call" | custom-call | tf_op jit(solution)/shard_map/scale_outputs/pallas_call | solution.py:436

commit v3 on v2

--- a/solution.py
+++ b/solution.py
@@ -11,8 +11,8 @@
 LANES = 128
 F32, BF16 = jnp.float32, jnp.bfloat16
 
-FIRST, START, MORE, HOP, PACE = 4, 2, 5, 2, 3
-CROSS, SPREAD, APART, TAKE = 2, 4, 4, 6
+START, HOP, PACE = 2, 2, 3
+CROSS, SPREAD, APART, TAKE = 1, 3, 4, 6
 
 
 def rows_dot(left, right):
@@ -151,10 +151,12 @@
     load_wd.wait()
     cot_move.wait_recv()
 
-    def act(k):
-        pa_out[:, lanes(k)] = cols_dot(tok[1, own_hf, :], wd[lanes(k), :]).astype(BF16)
-        pa_copy(k).start()
-        pa_own[:, lanes(k)] = cols_dot(tok[1, own_f, :], wd[lanes(k), :])
+    def act(j):
+        at = pl.ds(pl.multiple_of(j * 2 * LANES, 2 * LANES), 2 * LANES)
+        pa_out[:, at] = cols_dot(tok[1, own_hf, :], wd[at, :]).astype(BF16)
+        for n in range(2):
+            pa_copy(2 * j + n).start()
+        pa_own[:, at] = cols_dot(tok[1, own_f, :], wd[at, :])
 
     def pair(k):
         ox_copy(k).start()
@@ -234,6 +236,7 @@
         final(k, 1 - side, fc_s, inner).wait_recv()
         spread(k, 1 - side)
 
+    def forward_near(k):
         @pl.when(jnp.logical_not(middle))
         def _():
             final(k, side, fc_s, inner).wait_recv()
@@ -245,23 +248,42 @@
         moved(res, (1 - col, *at), fy_s, fy_r.at[k], other_y).wait_recv()
         up_ref[cols(w), lanes(p)] = res[(0, *at)].T
 
+    def grads_by(i):
+        fast = 2 * START + PACE + PACE * i
+        slow = 2 * START + 2 * PACE + i
+        return jnp.minimum(panels, jnp.where(
+            col == 1, jnp.minimum(fast, slow), 2 * START + i))
+
+    def acts_by(i):
+        return jnp.minimum(panels // 2, (grads_by(i + 1) + 2 - col) // 2)
+
     def when_in(i, end, body):
         @pl.when((i >= 0) & (i < end))
         def _():
             body(i)
 
-    each(0, FIRST, act)
+    act(0)
+
+    @pl.when(col == 1)
+    def _():
+        each(0, START, pair)
+        act(1)
 
     def ready(k):
         grad(k)
-        pair(k)
+
+        @pl.when(col == 0)
+        def _():
+            pair(k)
     each(0, START, ready)
 
     @pl.when(col == 1)
     def _():
         y_move(1).start()
-    act(FIRST)
-    more = FIRST + 1 + MORE
+
+    @pl.when(col == 0)
+    def _():
+        act(1)
 
     def far_arrived(w):
         remote(tok.at[1 - col, own_t, cols(w)], tok.at[col, far_t, cols(w)], yt_s.at[w],
@@ -276,18 +298,37 @@
 
     each(0, HOP, hop)
     far_move(0).wait_recv()
-    each(FIRST + 1, more, act)
-    each(START, START + PACE, grad)
+
+    each(2, acts_by(-1), act)
+    each(START, grads_by(-1), grad)
 
     furthest = SPREAD + APART * (mid - 1)
     take_lag = furthest + TAKE
 
     def spreading(k):
+        when_in(k - SPREAD - APART * depth, chunks, forward)
+        when_in(k - CROSS - APART * depth, chunks, forward_near)
         when_in(k - CROSS, chunks, cross)
-        when_in(k - SPREAD - APART * depth, chunks, forward)
         when_in(k - take_lag, chunks, take)
 
+    def feed(i):
+        when_in(i + HOP, panels, pair)
+
+        @pl.when(col == 1)
+        def _():
+            when_in(i + HOP, panels, hop)
+        each(acts_by(i - 1), acts_by(i), act)
+        each(grads_by(i - 1), grads_by(i), grad)
+
+        @pl.when(col == 0)
+        def _():
+            when_in(i + HOP, panels, hop)
+
     def main(i):
+        @pl.when(has_outer)
+        def _():
+            feed(i)
+
         @pl.when(i == 1)
         def _():
             far_arrived(1)
@@ -301,14 +342,12 @@
                 def _():
                     arrive(i)
             reduce(2 * i + n)
-
-            if n == 0:
-                for step in range(PACE):
-                    when_in(more + PACE * i + step, panels, act)
-                    when_in(START + PACE + PACE * i + step, panels, grad)
-                when_in(i + HOP, panels, pair)
-                when_in(i + HOP, panels, hop)
             spreading(2 * i + n)
+
+            if n == 1:
+                @pl.when(jnp.logical_not(has_outer))
+                def _():
+                    feed(i)
 
         @pl.when((col == 1) & (i >= panels // 2))
         def _():

time: 150 us -> 145 us (0.967)
  Pallas kernels: 149 us -> 145 us
    pallas_call x1, Pallas kernels: 143 us -> 138 us  [per_device(): pl.pallas_call(functools.partial(kernel, n_rep), name='ffn_backward', out...]
where the time goes in v3:
time: 145 us
  Pallas kernels  145 us (100%)
    pallas_call x1, Pallas kernels, per_device(): pl.pallas_call(functools.partial(kernel, n_rep), name='ffn_backward', out...  138 us
    pallas_call x1, Pallas kernels, per_device(): pl.pallas_call(functools.partial(scale_kernel, factor, pieces), name='sca...  6.2 us

profile of v3, /device:TPU:0, one launch (start us, length us, event | category | flops | bytes accessed | tf_op | source)
XLA Modules:
  0.0 145.3 jit_solution(15593220706518929656)
XLA Ops:
  0.6 138.5 %ffn_backward.1 = (bf16[256,1024]{1,0:T(8,128)(2,1)S(1)}, bf16[1024,2048]{1,0:T(8,128)(2,1)S(1)}, bf16[2,2048,1024]{2,1,0:T(8,128)(2,1)S(1)}) custom-call(bf16[256,1024]{1,0:T(8,128)(2,1)} %x_hbm.1, bf16[256,2048]{1,0:T(8,128)(2,1)} %pre_hbm.1, bf16[256,1024]{1,0:T(8,128)(2,1)} %cot_hbm.1, bf16[1024,2048]{1,0:T(8,128)(2,1)} %wu_hbm.1, bf16[2048,1024]{1,0:T(8,128)(2,1)} %wd_hbm.1), custom_call_target="tpu_custom_call" | custom-call | tf_op jit(solution)/shard_map/ffn_backward/pallas_call | solution.py:440
  139.1 6.2 %scale_outputs.1 = (bf16[256,1024]{1,0:T(8,128)(2,1)}, f32[1024,2048]{1,0:T(8,128)}, f32[2048,1024]{1,0:T(8,128)}) custom-call(bf16[256,1024]{1,0:T(8,128)(2,1)S(1)} %get-tuple-element.6.gi, bf16[1024,2048]{1,0:T(8,128)(2,1)S(1)} %get-tuple-element.7.up, bf16[2,2048,1024]{2,1,0:T(8,128)(2,1)S(1)} %get-tuple-element.8.res), custom_call_target="tpu_custom_call" | custom-call | tf_op jit(solution)/shard_map/scale_outputs/pallas_call | solution.py:475

commit v4 on v3

--- a/solution.py
+++ b/solution.py
@@ -13,6 +13,7 @@
 
 START, HOP, PACE = 2, 2, 3
 CROSS, SPREAD, APART, TAKE = 1, 3, 4, 6
+RELAY, LATE = 16, 9
 
 
 def rows_dot(left, right):
@@ -28,7 +29,7 @@
     gi_ref, up_ref, res,
     pre_ref, wu, wd, tok, hid, pa_own, pa_out, pa_in, gi_out, gi_in, part, out, inc,
     w_sem, tp_s, tp_r, yt_s, yt_r, ya_s, ya_r, ox_s, fx_s, act_r, gx_s, gx_r,
-    pa_s, pa_r, gi_s, gi_r, rs_s, rs_r, fc_s, fo_s, fz_r, fy_s, fy_r,
+    pa_s, pa_r, gi_s, gi_r, rs_s, rs_r, fc_s, fo_s, fz_r, fy_s, fy_r, rc_s, ro_s, rz_r,
 ):
     half, hidden = pre_ref.shape
     width = wd.shape[1]
@@ -68,11 +69,13 @@
     barrier = pltpu.get_barrier_semaphore()
     for dev in (outer, inner, other_y, other_fs, other_tp):
         pl.semaphore_signal(barrier, inc=1, device_id=dev, device_id_type=MESH)
+    first = pl.ds(0, 2 * LANES)
+    rest = pl.ds(2 * LANES, hidden - 2 * LANES)
     held = ((cot_hbm, tok.at[1, own_t]), (x_hbm, tok.at[0, own_t]), (pre_hbm, pre_ref),
-            (wd_hbm, wd), (wu_hbm, wu))
+            (wd_hbm.at[first], wd.at[first]), (wd_hbm.at[rest], wd.at[rest]), (wu_hbm, wu))
     loads = [pltpu.make_async_copy(src, dst, w_sem.at[i]) for i, (src, dst) in enumerate(held)]
-    load_cot, load_x, load_pre, load_wd, load_wu = loads
-    for load in loads:
+    load_cot, load_x, load_pre, load_first, load_rest, load_wu = loads
+    for load in loads[:4]:
         load.start()
     load_cot.wait()
     load_x.wait()
@@ -147,8 +150,9 @@
     @pl.when(col == 0)
     def _():
         y_move(1).start()
-    each(2, panels, own_square)
-    load_wd.wait()
+    load_rest.start()
+    load_wu.start()
+    load_first.wait()
     cot_move.wait_recv()
 
     def act(j):
@@ -217,11 +221,20 @@
             else:
                 rs_copy(k, s).start()
 
+    def relayed(k):
+        return k % RELAY == RELAY // 2
+
     def spread(k, s):
         @pl.when(has_outer)
         def _():
             final(k, s, fo_s, outer).start()
-        final_y(k, s).start()
+
+    def spread_y(k, s):
+        spread(k, s)
+
+        @pl.when(jnp.logical_not(relayed(k)))
+        def _():
+            final_y(k, s).start()
 
     def cross(k):
         @pl.when(middle)
@@ -231,28 +244,59 @@
             res[(col, *at)] = (out[at].astype(F32) + inc[(1, *at)].astype(F32)).astype(BF16)
             final(k, side, fc_s, inner).start()
             spread(k, side)
+            final_y(k, side).start()
 
     def forward(k):
         final(k, 1 - side, fc_s, inner).wait_recv()
-        spread(k, 1 - side)
+        spread_y(k, 1 - side)
 
     def forward_near(k):
         @pl.when(jnp.logical_not(middle))
         def _():
             final(k, side, fc_s, inner).wait_recv()
-            spread(k, side)
+            spread_y(k, side)
+
+    def relay(k, s, sem, dev):
+        return moved(res, (1 - col, *piece(k, s)), sem, rz_r.at[k // RELAY, s], dev)
+
+    def relay_out(k, s):
+        @pl.when(has_outer)
+        def _():
+            relay(k, s, ro_s, outer).start()
+
+    def relay_near(k):
+        @pl.when(relayed(k))
+        def _():
+            @pl.when(middle)
+            def _():
+                moved(res, (1 - col, *piece(k, side)), fy_s, fy_r.at[k], other_y).wait_recv()
+                relay(k, side, rc_s, inner).start()
+
+            @pl.when(jnp.logical_not(middle))
+            def _():
+                relay(k, side, rc_s, inner).wait_recv()
+            relay_out(k, side)
+
+    def relay_far(k):
+        @pl.when(relayed(k))
+        def _():
+            relay(k, 1 - side, rc_s, inner).wait_recv()
+            relay_out(k, 1 - side)
 
     def take(k):
         p, w = where_is(k)
         at = (lanes(p), cols(w))
-        moved(res, (1 - col, *at), fy_s, fy_r.at[k], other_y).wait_recv()
+
+        @pl.when(jnp.logical_not(relayed(k)))
+        def _():
+            moved(res, (1 - col, *at), fy_s, fy_r.at[k], other_y).wait_recv()
         up_ref[cols(w), lanes(p)] = res[(0, *at)].T
 
     def grads_by(i):
         fast = 2 * START + PACE + PACE * i
         slow = 2 * START + 2 * PACE + i
         return jnp.minimum(panels, jnp.where(
-            col == 1, jnp.minimum(fast, slow), 2 * START + i))
+            col == 1, jnp.minimum(fast, slow), START + 1 + i))
 
     def acts_by(i):
         return jnp.minimum(panels // 2, (grads_by(i + 1) + 2 - col) // 2)
@@ -263,6 +307,8 @@
             body(i)
 
     act(0)
+    each(2, panels, own_square)
+    load_rest.wait()
 
     @pl.when(col == 1)
     def _():
@@ -280,10 +326,6 @@
     @pl.when(col == 1)
     def _():
         y_move(1).start()
-
-    @pl.when(col == 0)
-    def _():
-        act(1)
 
     def far_arrived(w):
         remote(tok.at[1 - col, own_t, cols(w)], tok.at[col, far_t, cols(w)], yt_s.at[w],
@@ -299,29 +341,35 @@
     each(0, HOP, hop)
     far_move(0).wait_recv()
 
-    each(2, acts_by(-1), act)
+    each(2 - jnp.where(col == 0, 1, 0), acts_by(-1), act)
     each(START, grads_by(-1), grad)
 
     furthest = SPREAD + APART * (mid - 1)
-    take_lag = furthest + TAKE
+    take_lag = furthest + max(TAKE, LATE + 2 * CROSS + 1 - SPREAD)
 
     def spreading(k):
         when_in(k - SPREAD - APART * depth, chunks, forward)
         when_in(k - CROSS - APART * depth, chunks, forward_near)
         when_in(k - CROSS, chunks, cross)
+        when_in(k - LATE - APART * depth, chunks, relay_near)
+        when_in(k - LATE - 2 * CROSS - APART * depth, chunks, relay_far)
         when_in(k - take_lag, chunks, take)
 
     def feed(i):
-        when_in(i + HOP, panels, pair)
-
         @pl.when(col == 1)
         def _():
+            when_in(i + HOP, panels, pair)
             when_in(i + HOP, panels, hop)
         each(acts_by(i - 1), acts_by(i), act)
+
+        @pl.when(i == 0)
+        def _():
+            far_arrived(1)
         each(grads_by(i - 1), grads_by(i), grad)
 
         @pl.when(col == 0)
         def _():
+            when_in(i + HOP, panels, pair)
             when_in(i + HOP, panels, hop)
 
     def main(i):
@@ -331,7 +379,6 @@
 
         @pl.when(i == 1)
         def _():
-            far_arrived(1)
             far_move(1).wait_recv()
         for n in range(2):
             @pl.when(i == 0)
@@ -355,31 +402,39 @@
                 gx_copy(2 * (i - panels // 2) + n).start()
 
     each(0, panels, main)
-    each(chunks, chunks + 2, spreading)
     load_wu.wait()
-
-    @pl.when(col == 1)
-    def _():
-        moved(hid, (0, own_f), gx_s, gx_r, other_fs).wait_recv()
-
     strip = min(2 * LANES, width)
 
     def input_out(n):
         at = pl.ds(pl.multiple_of(n * strip, strip), strip)
         gi_out[:, at] = cols_dot(hid[0, own_ht, :], wu[at, :]).astype(BF16)
-    each(0, width // strip, input_out)
-    gi_move = remote(gi_out, gi_in, gi_s, gi_r, other_tp)
-    gi_move.start()
-    each(chunks + 2, chunks + 6, spreading)
-
     def input_own(n):
         at = pl.ds(pl.multiple_of(n * strip, strip), strip)
         mine = cols_dot(hid[0, own_t, :], wu[at, :]).astype(BF16).astype(F32)
         gi_ref[:, at] = mine.astype(BF16)
-    each(0, width // strip, input_own)
+    strips = width // strip
+    gi_move = remote(gi_out, gi_in, gi_s, gi_r, other_tp)
+
+    def finish(n):
+        spreading(chunks + n)
+        m = n - jnp.where(has_outer, SPREAD, 0)
+
+        @pl.when((col == 1) & (m == 0))
+        def _():
+            moved(hid, (0, own_f), gx_s, gx_r, other_fs).wait_recv()
+
+        for h in range(2):
+            when_in(2 * m + h, strips, input_out)
+        for h in range(2):
+            when_in(2 * m + h - strips, strips, input_own)
+
+        @pl.when(m == strips // 2 - 1)
+        def _():
+            gi_move.start()
+    each(0, SPREAD + strips, finish)
+    each(chunks + SPREAD + strips, chunks + take_lag, spreading)
     gi_move.wait_recv()
     gi_ref[...] = (gi_ref[...].astype(F32) + gi_in[...].astype(F32)).astype(BF16)
-    each(chunks + 6, chunks + take_lag, spreading)
 
     for move in (y_move(0), y_move(1), cot_move, far_move(0), far_move(1), gi_move):
         move.wait_send()
@@ -388,7 +443,8 @@
     moved(hid, (1 - col, own_f), ya_s, ya_r.at[0], other_y).wait_send()
     moved(hid, (col, own_f), ox_s, act_r.at[0], other_fs).wait_send()
     moved(hid, (col, far_f), fx_s, act_r.at[0], other_fs).wait_send()
-    moved(res, (col,), fy_s, fy_r.at[0], other_y).wait_send()
+    relays = len(range(RELAY // 2, chunks, RELAY))
+    passed = relays * sub // 2
 
     @pl.when(col == 0)
     def _():
@@ -402,14 +458,20 @@
     def _():
         remote(out.at[some], inc.at[1, some], rs_s, rs_r.at[2, 0], inner).wait_send()
         moved(res, (col, some), fc_s, fz_r.at[0, 0], inner).wait_send()
+        kept = pl.ds(0, hidden - passed)
+        moved(res, (col, kept), fy_s, fy_r.at[0], other_y).wait_send()
+        moved(res, (1 - col, pl.ds(0, passed)), rc_s, rz_r.at[0, 0], inner).wait_send()
 
     @pl.when(jnp.logical_not(middle))
     def _():
         remote(out, inc.at[0], rs_s, rs_r.at[0, 0], inner).wait_send()
+        kept = pl.ds(0, hidden - 2 * passed)
+        moved(res, (col, kept), fy_s, fy_r.at[0], other_y).wait_send()
 
     @pl.when(has_outer)
     def _():
         moved(res, (col,), fo_s, fz_r.at[0, 0], outer).wait_send()
+        moved(res, (1 - col, pl.ds(0, 2 * passed)), ro_s, rz_r.at[0, 0], outer).wait_send()
 
 
 def scale_kernel(factor, pieces, gi, up, res, gi_out, up_out, down_out, up_wide, down_wide,
@@ -461,10 +523,11 @@
             pltpu.VMEM((LANES, width // 2), F32),
             pltpu.VMEM((hidden, width), BF16),
             pltpu.VMEM((2, hidden, width), BF16),
-            dma((5,)), dma((4,)), dma((4,)), dma((2,)), dma((2,)),
+            dma((6,)), dma((4,)), dma((4,)), dma((2,)), dma((2,)),
             dma, one, dma, dma, one, dma, dma,
             dma, one, dma, dma,
             dma, dma((3, chunks)), dma, dma, dma((chunks, 2)), dma, dma((chunks,)),
+            dma, dma, dma((-(-chunks // RELAY), 2)),
         ],
         compiler_params=pltpu.CompilerParams(
             collective_id=0, has_side_effects=True, vmem_limit_bytes=48 * 2**20

time: 145 us -> 142 us (0.979)
  Pallas kernels: 145 us -> 141 us
    pallas_call x1, Pallas kernels: 138 us -> 135 us  [per_device(): pl.pallas_call(functools.partial(kernel, n_rep), name='ffn_backward', out...]
where the time goes in v4:
time: 142 us
  Pallas kernels  141 us (99%)
    pallas_call x1, Pallas kernels, per_device(): pl.pallas_call(functools.partial(kernel, n_rep), name='ffn_backward', out...  135 us
    pallas_call x1, Pallas kernels, per_device(): pl.pallas_call(functools.partial(scale_kernel, factor, pieces), name='sca...  6.2 us

profile of v4, /device:TPU:0, one launch (start us, length us, event | category | flops | bytes accessed | tf_op | source)
XLA Modules:
  0.0 142.0 jit_solution(6888483345988942934)
XLA Ops:
  0.6 135.2 %ffn_backward.1 = (bf16[256,1024]{1,0:T(8,128)(2,1)S(1)}, bf16[1024,2048]{1,0:T(8,128)(2,1)S(1)}, bf16[2,2048,1024]{2,1,0:T(8,128)(2,1)S(1)}) custom-call(bf16[256,1024]{1,0:T(8,128)(2,1)} %x_hbm.1, bf16[256,2048]{1,0:T(8,128)(2,1)} %pre_hbm.1, bf16[256,1024]{1,0:T(8,128)(2,1)} %cot_hbm.1, bf16[1024,2048]{1,0:T(8,128)(2,1)} %wu_hbm.1, bf16[2048,1024]{1,0:T(8,128)(2,1)} %wd_hbm.1), custom_call_target="tpu_custom_call" | custom-call | tf_op jit(solution)/shard_map/ffn_backward/pallas_call | solution.py:502
  135.8 6.2 %scale_outputs.1 = (bf16[256,1024]{1,0:T(8,128)(2,1)}, f32[1024,2048]{1,0:T(8,128)}, f32[2048,1024]{1,0:T(8,128)}) custom-call(bf16[256,1024]{1,0:T(8,128)(2,1)S(1)} %get-tuple-element.6.gi, bf16[1024,2048]{1,0:T(8,128)(2,1)S(1)} %get-tuple-element.7.up, bf16[2,2048,1024]{2,1,0:T(8,128)(2,1)S(1)} %get-tuple-element.8.res), custom_call_target="tpu_custom_call" | custom-call | tf_op jit(solution)/shard_map/scale_outputs/pallas_call | solution.py:538

commit v5 on v4

--- a/solution.py
+++ b/solution.py
@@ -13,7 +13,7 @@
 
 START, HOP, PACE = 2, 2, 3
 CROSS, SPREAD, APART, TAKE = 1, 3, 4, 6
-RELAY, LATE = 16, 9
+RELAY, LATE = (32, 16), 9
 
 
 def rows_dot(left, right):
@@ -22,6 +22,11 @@
 
 def cols_dot(left, right):
     return lax.dot_general(left, right, (((1,), (1,)), ((), ())), preferred_element_type=F32)
+
+
+def turn_of(n_rep, chunks):
+    furthest = SPREAD + APART * (n_rep // 4 - 1)
+    return min(chunks, 1 << (furthest + TAKE).bit_length())
 
 
 def kernel(
@@ -95,6 +100,8 @@
         p, w = where_is(k)
         return pl.ds(pl.multiple_of(p * LANES + s * sub, sub), sub), cols(w)
 
+    turn = turn_of(n_rep, chunks)
+
     def moved(ref, at, s, r, dev):
         return remote(ref.at[at], ref.at[at], s, r, dev)
 
@@ -180,17 +187,22 @@
                ya_r.at[k], other_y).wait_recv()
         fx_copy(k).start()
 
-    def rs_copy(k, s):
+    def rs_copy(k, s, recv):
         slot = jnp.where(middle, 1, 0)
         return remote(out.at[piece(k, s)], inc.at[(slot, *piece(k, s))], rs_s,
-                      rs_r.at[jnp.where(middle, 2, s), k], inner)
-
-    def rs_wait(slot, k, s):
-        remote(out.at[piece(k, s)], inc.at[(slot, *piece(k, s))], rs_s,
-               rs_r.at[2 if slot else s, k], inner).wait_recv()
+                      recv.at[k % turn, s], inner)
+
+    def rs_start(k, s):
+        @pl.when(middle)
+        def _():
+            rs_copy(k, s, fz_r).start()
+
+        @pl.when(jnp.logical_not(middle))
+        def _():
+            rs_copy(k, s, rs_r).start()
 
     def final(k, s, sem, dev):
-        return moved(res, (col, *piece(k, s)), sem, fz_r.at[k, s], dev)
+        return moved(res, (col, *piece(k, s)), sem, fz_r.at[k % turn, s], dev)
 
     def final_y(k, s):
         return moved(res, (col, *piece(k, s)), fy_s, fy_r.at[k], other_y)
@@ -207,7 +219,7 @@
 
             @pl.when(has_outer)
             def _():
-                rs_wait(0, k, s)
+                rs_copy(k, s, rs_r).wait_recv()
                 out[at] = (mine + inc[(0, *at)].astype(F32)).astype(BF16)
 
             @pl.when(jnp.logical_not(has_outer))
@@ -217,12 +229,13 @@
             if s is side:
                 @pl.when(jnp.logical_not(middle))
                 def _():
-                    rs_copy(k, s).start()
+                    rs_copy(k, s, rs_r).start()
             else:
-                rs_copy(k, s).start()
-
-    def relayed(k):
-        return k % RELAY == RELAY // 2
+                rs_start(k, s)
+
+    def relayed(k, c):
+        every = jnp.where(c == 0, RELAY[0], RELAY[1])
+        return k % every == every // 2
 
     def spread(k, s):
         @pl.when(has_outer)
@@ -232,7 +245,7 @@
     def spread_y(k, s):
         spread(k, s)
 
-        @pl.when(jnp.logical_not(relayed(k)))
+        @pl.when(jnp.logical_not(relayed(k, col)))
         def _():
             final_y(k, s).start()
 
@@ -240,7 +253,7 @@
         @pl.when(middle)
         def _():
             at = piece(k, side)
-            rs_wait(1, k, side)
+            rs_copy(k, side, fz_r).wait_recv()
             res[(col, *at)] = (out[at].astype(F32) + inc[(1, *at)].astype(F32)).astype(BF16)
             final(k, side, fc_s, inner).start()
             spread(k, side)
@@ -257,7 +270,7 @@
             spread_y(k, side)
 
     def relay(k, s, sem, dev):
-        return moved(res, (1 - col, *piece(k, s)), sem, rz_r.at[k // RELAY, s], dev)
+        return moved(res, (1 - col, *piece(k, s)), sem, rz_r.at[k // min(RELAY), s], dev)
 
     def relay_out(k, s):
         @pl.when(has_outer)
@@ -265,7 +278,7 @@
             relay(k, s, ro_s, outer).start()
 
     def relay_near(k):
-        @pl.when(relayed(k))
+        @pl.when(relayed(k, 1 - col))
         def _():
             @pl.when(middle)
             def _():
@@ -278,7 +291,7 @@
             relay_out(k, side)
 
     def relay_far(k):
-        @pl.when(relayed(k))
+        @pl.when(relayed(k, 1 - col))
         def _():
             relay(k, 1 - side, rc_s, inner).wait_recv()
             relay_out(k, 1 - side)
@@ -287,13 +300,14 @@
         p, w = where_is(k)
         at = (lanes(p), cols(w))
 
-        @pl.when(jnp.logical_not(relayed(k)))
+        @pl.when(jnp.logical_not(relayed(k, 1 - col)))
         def _():
             moved(res, (1 - col, *at), fy_s, fy_r.at[k], other_y).wait_recv()
         up_ref[cols(w), lanes(p)] = res[(0, *at)].T
 
     def grads_by(i):
-        fast = 2 * START + PACE + PACE * i
+        pace = jnp.where(has_outer, PACE, START)
+        fast = 2 * START + jnp.where(i < 0, 0, PACE + pace * i)
         slow = 2 * START + 2 * PACE + i
         return jnp.minimum(panels, jnp.where(
             col == 1, jnp.minimum(fast, slow), START + 1 + i))
@@ -443,9 +457,6 @@
     moved(hid, (1 - col, own_f), ya_s, ya_r.at[0], other_y).wait_send()
     moved(hid, (col, own_f), ox_s, act_r.at[0], other_fs).wait_send()
     moved(hid, (col, far_f), fx_s, act_r.at[0], other_fs).wait_send()
-    relays = len(range(RELAY // 2, chunks, RELAY))
-    passed = relays * sub // 2
-
     @pl.when(col == 0)
     def _():
         x_move.wait_send()
@@ -456,22 +467,41 @@
 
     @pl.when(middle)
     def _():
-        remote(out.at[some], inc.at[1, some], rs_s, rs_r.at[2, 0], inner).wait_send()
+        remote(out.at[some], inc.at[1, some], rs_s, rs_r.at[0, 0], inner).wait_send()
         moved(res, (col, some), fc_s, fz_r.at[0, 0], inner).wait_send()
-        kept = pl.ds(0, hidden - passed)
-        moved(res, (col, kept), fy_s, fy_r.at[0], other_y).wait_send()
-        moved(res, (1 - col, pl.ds(0, passed)), rc_s, rz_r.at[0, 0], inner).wait_send()
 
     @pl.when(jnp.logical_not(middle))
     def _():
         remote(out, inc.at[0], rs_s, rs_r.at[0, 0], inner).wait_send()
-        kept = pl.ds(0, hidden - 2 * passed)
-        moved(res, (col, kept), fy_s, fy_r.at[0], other_y).wait_send()
 
     @pl.when(has_outer)
     def _():
         moved(res, (col,), fo_s, fz_r.at[0, 0], outer).wait_send()
-        moved(res, (1 - col, pl.ds(0, 2 * passed)), ro_s, rz_r.at[0, 0], outer).wait_send()
+
+    def relay_sent(c):
+        passed = [len(range(n // 2, chunks, n)) * sub // 2 for n in RELAY]
+
+        @pl.when(middle)
+        def _():
+            kept = pl.ds(0, hidden - passed[c])
+            moved(res, (c, kept), fy_s, fy_r.at[0], other_y).wait_send()
+            some = pl.ds(0, passed[1 - c])
+            moved(res, (1 - c, some), rc_s, rz_r.at[0, 0], inner).wait_send()
+
+        @pl.when(jnp.logical_not(middle))
+        def _():
+            kept = pl.ds(0, hidden - 2 * passed[c])
+            moved(res, (c, kept), fy_s, fy_r.at[0], other_y).wait_send()
+
+        @pl.when(has_outer)
+        def _():
+            some = pl.ds(0, 2 * passed[1 - c])
+            moved(res, (1 - c, some), ro_s, rz_r.at[0, 0], outer).wait_send()
+
+    for c in range(2):
+        @pl.when(col == c)
+        def _():
+            relay_sent(c)
 
 
 def scale_kernel(factor, pieces, gi, up, res, gi_out, up_out, down_out, up_wide, down_wide,
@@ -498,6 +528,7 @@
     vmem = pl.BlockSpec(memory_space=pltpu.VMEM)
     anywhere = pl.BlockSpec(memory_space=pl.ANY)
     chunks = 2 * panels
+    turn = turn_of(n_rep, chunks)
     one = dma((panels,))
     grad_inputs, grad_up, result = pl.pallas_call(
         functools.partial(kernel, n_rep),
@@ -526,8 +557,8 @@
             dma((6,)), dma((4,)), dma((4,)), dma((2,)), dma((2,)),
             dma, one, dma, dma, one, dma, dma,
             dma, one, dma, dma,
-            dma, dma((3, chunks)), dma, dma, dma((chunks, 2)), dma, dma((chunks,)),
-            dma, dma, dma((-(-chunks // RELAY), 2)),
+            dma, dma((turn, 2)), dma, dma, dma((turn, 2)), dma, dma((chunks,)),
+            dma, dma, dma((-(-chunks // min(RELAY)), 2)),
         ],
         compiler_params=pltpu.CompilerParams(
             collective_id=0, has_side_effects=True, vmem_limit_bytes=48 * 2**20

time: 142 us -> 140 us (0.986)
  Pallas kernels: 141 us -> 139 us
    pallas_call x1, Pallas kernels: 135 us -> 133 us  [per_device(): pl.pallas_call(functools.partial(kernel, n_rep), name='ffn_backward', out...]
where the time goes in v5:
time: 140 us; the launch traced here: 139 us
  Pallas kernels  139 us (99%)
    pallas_call x1, Pallas kernels, per_device(): pl.pallas_call(functools.partial(kernel, n_rep), name='ffn_backward', out...  133 us
    pallas_call x1, Pallas kernels, per_device(): pl.pallas_call(functools.partial(scale_kernel, factor, pieces), name='sca...  6.2 us

profile of v5, /device:TPU:0, one launch (start us, length us, event | category | flops | bytes accessed | tf_op | source)
XLA Modules:
  0.0 139.4 jit_solution(2561493760434295520)
XLA Ops:
  0.6 132.5 %ffn_backward.1 = (bf16[256,1024]{1,0:T(8,128)(2,1)S(1)}, bf16[1024,2048]{1,0:T(8,128)(2,1)S(1)}, bf16[2,2048,1024]{2,1,0:T(8,128)(2,1)S(1)}) custom-call(bf16[256,1024]{1,0:T(8,128)(2,1)} %x_hbm.1, bf16[256,2048]{1,0:T(8,128)(2,1)} %pre_hbm.1, bf16[256,1024]{1,0:T(8,128)(2,1)} %cot_hbm.1, bf16[1024,2048]{1,0:T(8,128)(2,1)} %wu_hbm.1, bf16[2048,1024]{1,0:T(8,128)(2,1)} %wd_hbm.1), custom_call_target="tpu_custom_call" | custom-call | tf_op jit(solution)/shard_map/ffn_backward/pallas_call | solution.py:533
  133.2 6.2 %scale_outputs.1 = (bf16[256,1024]{1,0:T(8,128)(2,1)}, f32[1024,2048]{1,0:T(8,128)}, f32[2048,1024]{1,0:T(8,128)}) custom-call(bf16[256,1024]{1,0:T(8,128)(2,1)S(1)} %get-tuple-element.6.gi, bf16[1024,2048]{1,0:T(8,128)(2,1)S(1)} %get-tuple-element.7.up, bf16[2,2048,1024]{2,1,0:T(8,128)(2,1)S(1)} %get-tuple-element.8.res), custom_call_target="tpu_custom_call" | custom-call | tf_op jit(solution)/shard_map/scale_outputs/pallas_call | solution.py:569

commit v6 on v5

--- a/solution.py
+++ b/solution.py
@@ -13,7 +13,7 @@
 
 START, HOP, PACE = 2, 2, 3
 CROSS, SPREAD, APART, TAKE = 1, 3, 4, 6
-RELAY, LATE = (32, 16), 9
+RELAY, LATE = (32, 16), 11
 
 
 def rows_dot(left, right):
@@ -164,8 +164,9 @@
 
     def act(j):
         at = pl.ds(pl.multiple_of(j * 2 * LANES, 2 * LANES), 2 * LANES)
-        pa_out[:, at] = cols_dot(tok[1, own_hf, :], wd[at, :]).astype(BF16)
         for n in range(2):
+            pa_out[:, lanes(2 * j + n)] = cols_dot(
+                tok[1, own_hf, :], wd[lanes(2 * j + n), :]).astype(BF16)
             pa_copy(2 * j + n).start()
         pa_own[:, at] = cols_dot(tok[1, own_f, :], wd[at, :])
 
@@ -307,7 +308,7 @@
 
     def grads_by(i):
         pace = jnp.where(has_outer, PACE, START)
-        fast = 2 * START + jnp.where(i < 0, 0, PACE + pace * i)
+        fast = 2 * START + jnp.where(i < 0, 0, START + pace * i)
         slow = 2 * START + 2 * PACE + i
         return jnp.minimum(panels, jnp.where(
             col == 1, jnp.minimum(fast, slow), START + 1 + i))

time: 140 us -> 139 us (level)
  no operation moved by 1% of the time
where the time goes in v6:
time: 139 us
  Pallas kernels  138 us (99%)
    pallas_call x1, Pallas kernels, per_device(): pl.pallas_call(functools.partial(kernel, n_rep), name='ffn_backward', out...  132 us
    pallas_call x1, Pallas kernels, per_device(): pl.pallas_call(functools.partial(scale_kernel, factor, pieces), name='sca...  6.2 us

profile of v6, /device:TPU:0, one launch (start us, length us, event | category | flops | bytes accessed | tf_op | source)
XLA Modules:
  0.0 138.8 jit_solution(9174237858215923156)
XLA Ops:
  0.6 132.0 %ffn_backward.1 = (bf16[256,1024]{1,0:T(8,128)(2,1)S(1)}, bf16[1024,2048]{1,0:T(8,128)(2,1)S(1)}, bf16[2,2048,1024]{2,1,0:T(8,128)(2,1)S(1)}) custom-call(bf16[256,1024]{1,0:T(8,128)(2,1)} %x_hbm.1, bf16[256,2048]{1,0:T(8,128)(2,1)} %pre_hbm.1, bf16[256,1024]{1,0:T(8,128)(2,1)} %cot_hbm.1, bf16[1024,2048]{1,0:T(8,128)(2,1)} %wu_hbm.1, bf16[2048,1024]{1,0:T(8,128)(2,1)} %wd_hbm.1), custom_call_target="tpu_custom_call" | custom-call | tf_op jit(solution)/shard_map/ffn_backward/pallas_call | solution.py:534
  132.6 6.2 %scale_outputs.1 = (bf16[256,1024]{1,0:T(8,128)(2,1)}, f32[1024,2048]{1,0:T(8,128)}, f32[2048,1024]{1,0:T(8,128)}) custom-call(bf16[256,1024]{1,0:T(8,128)(2,1)S(1)} %get-tuple-element.6.gi, bf16[1024,2048]{1,0:T(8,128)(2,1)S(1)} %get-tuple-element.7.up, bf16[2,2048,1024]{2,1,0:T(8,128)(2,1)S(1)} %get-tuple-element.8.res), custom_call_target="tpu_custom_call" | custom-call | tf_op jit(solution)/shard_map/scale_outputs/pallas_call | solution.py:570
